TPU v7x, 32 devices: a whole 2x2x4 slice. The times are simulated.
32 devices in a mesh: ep: 16 (over z, y, x), tp: 2 (over core).
Axes of the slice: x: 2, y: 2, z: 4, core: 2. Of those that a mesh axis runs over, the one named last changes fastest.
Arguments:
- tokens: bfloat16 [256, 2048], P('ep'), may hold values from -6 to 6
- norm_attn: float32 [2048], replicated, may hold values from 0.1 to 1.9
- w_query: bfloat16 [2048, 2048], P(None, 'tp'), may hold values from -0.125 to 0.125
- w_key: bfloat16 [2048, 256], P(None, 'tp'), may hold values from -0.125 to 0.125
- w_value: bfloat16 [2048, 256], P(None, 'tp'), may hold values from -0.125 to 0.125
- w_out: bfloat16 [2048, 2048], P('tp'), may hold values from -0.125 to 0.125
- attn_bias: float32 [32], P('tp'), may hold values from -7 to -1
- cache_keys: bfloat16 [256, 1024, 256], P('ep', None, 'tp'), may hold values from -6 to 6
- cache_values: bfloat16 [256, 1024, 256], P('ep', None, 'tp'), may hold values from -6 to 6
- lengths: int32 [256], P('ep'), may hold values from 256 to 1024
- norm_ffn: float32 [2048], replicated, may hold values from 0.1 to 1.9
- expert_gate: bfloat16 [2048, 57344], P(None, ('ep', 'tp')), may hold values from -0.125 to 0.125
- expert_up: bfloat16 [2048, 57344], P(None, ('ep', 'tp')), may hold values from -0.125 to 0.125
- expert_down: bfloat16 [57344, 2048], P(('ep', 'tp')), may hold values from -0.0625 to 0.0625
- dense_gate_w: bfloat16 [2048, 7168], P(None, 'ep'), may hold values from -0.125 to 0.125
- dense_up_w: bfloat16 [2048, 7168], P(None, 'ep'), may hold values from -0.125 to 0.125
- dense_down_w: bfloat16 [7168, 2048], P('ep'), may hold values from -0.0625 to 0.0625
- dense_mix: bfloat16 [2048], replicated, may hold values from -0.125 to 0.125
- routes: int32 [256, 2], P(('ep', 'tp')), may hold values from 0 to 7, all different within a row; in each aligned block of 8 rows (0 to 7, 8 to 15, ...) at most 3 rows name the same one
- route_weights: bfloat16 [256, 2], P(('ep', 'tp')), may hold values from 0.19921875 to 1
Outputs:
- layer_out: bfloat16 [256, 2048], P(('ep', 'tp'))
- new_keys: bfloat16 [256, 256], P('ep', 'tp')
- new_values: bfloat16 [256, 256], P('ep', 'tp')
Inputs may be any that keep to these rules, and one draw needn't show every extreme that they name: `routes`: in each aligned block of 8 rows (the rows of one device) no expert is named by more than 3 rows, a bound that some block reaches; a row names 2 different experts.
All inputs are finite; a program needn't handle non-finite values.
Results may differ from a plain program's by a relative error of at most 0.015.
Values may be sent and summed in bfloat16 or wider, within the bound.
A program may use at most 128 MiB of HBM per device.

v0:
```python
import jax
import jax.numpy as jnp
from jax import lax
from jax.sharding import PartitionSpec as P

HEAD_DIM = 64
EXPERTS = 8
TOP = 2
EPSILON = 1e-06


def normed_rows(values, gain):
    widened = values.astype(jnp.float32)
    scale = lax.rsqrt(jnp.mean(widened * widened, axis=-1, keepdims=True) + EPSILON)
    return (widened * scale * gain).astype(jnp.bfloat16)


def later_sums(log_keep):
    cache_len = log_keep.shape[-1]
    block_len = 128
    block_count = cache_len // block_len
    lead = log_keep.shape[:-1]
    blocked = log_keep.reshape(lead + (block_count, block_len))
    rows_in = lax.broadcasted_iota(jnp.int32, (block_len, block_len), 0)
    cols_in = lax.broadcasted_iota(jnp.int32, (block_len, block_len), 1)
    upper = (rows_in >= cols_in).astype(jnp.float32)
    within = jnp.einsum("...nj,ji->...ni", blocked, upper, precision=lax.Precision.HIGHEST)
    totals = within[..., 0]
    rows_out = lax.broadcasted_iota(jnp.int32, (block_count, block_count), 0)
    cols_out = lax.broadcasted_iota(jnp.int32, (block_count, block_count), 1)
    beyond = (rows_out > cols_out).astype(jnp.float32)
    following = jnp.einsum("...m,mn->...n", totals, beyond, precision=lax.Precision.HIGHEST)
    inclusive = within + following[..., None]
    return (inclusive - blocked).reshape(log_keep.shape)


def running_ranks(present):
    count = present.shape[-1]
    rows_in = lax.broadcasted_iota(jnp.int32, (count, count), 0)
    cols_in = lax.broadcasted_iota(jnp.int32, (count, count), 1)
    lower = (rows_in <= cols_in).astype(jnp.float32)
    totals = jnp.einsum(
        "...j,ji->...i", present.astype(jnp.float32), lower, precision=lax.Precision.HIGHEST
    )
    return totals.astype(jnp.int32) - 1


def shards(
    tokens,
    norm_attn,
    w_query,
    w_key,
    w_value,
    w_out,
    attn_bias,
    cache_keys,
    cache_values,
    lengths,
    norm_ffn,
    expert_gate,
    expert_up,
    expert_down,
    dense_gate_w,
    dense_up_w,
    dense_down_w,
    dense_mix,
    routes,
    route_weights,
):
    seq_count = tokens.shape[0]
    cache_len = cache_keys.shape[1]
    group_count = cache_keys.shape[2] // HEAD_DIM
    repeat = w_query.shape[1] // (group_count * HEAD_DIM)
    normed = normed_rows(tokens, norm_attn)
    query = jnp.dot(normed, w_query, preferred_element_type=jnp.float32).astype(jnp.bfloat16)
    new_keys = jnp.dot(normed, w_key, preferred_element_type=jnp.float32).astype(jnp.bfloat16)
    new_values = jnp.dot(normed, w_value, preferred_element_type=jnp.float32).astype(jnp.bfloat16)
    query_heads = query.reshape(seq_count, group_count, repeat, HEAD_DIM)
    key_heads = cache_keys.reshape(seq_count, cache_len, group_count, HEAD_DIM)
    value_heads = cache_values.reshape(seq_count, cache_len, group_count, HEAD_DIM)
    scores = jnp.einsum(
        "bgrd,bsgd->bgrs", query_heads, key_heads, preferred_element_type=jnp.float32
    ) * HEAD_DIM ** (-0.5)
    scores = scores + attn_bias.reshape(group_count, repeat)[None, :, :, None]
    places = lax.broadcasted_iota(jnp.int32, (seq_count, cache_len), 1)
    visible = (places < lengths[:, None])[:, None, None, :]
    log_keep = jnp.where(visible, jax.nn.log_sigmoid(-scores), 0.0)
    after = later_sums(log_keep)
    weight = jnp.where(visible, jnp.exp(jax.nn.log_sigmoid(scores) + after), 0.0).astype(
        jnp.bfloat16
    )
    heads_out = jnp.einsum(
        "bgrs,bsgd->bgrd", weight, value_heads, preferred_element_type=jnp.float32
    )
    heads_out = heads_out.astype(jnp.bfloat16).reshape(seq_count, group_count * repeat * HEAD_DIM)
    partial_value = jnp.dot(heads_out, w_out, preferred_element_type=jnp.float32)
    attn_sum = lax.psum_scatter(
        partial_value.astype(jnp.bfloat16), "tp", scatter_dimension=0, tiled=True
    ).astype(jnp.float32)
    row_count = seq_count // lax.axis_size("tp")
    capacity = (row_count * TOP + EXPERTS - 1) // EXPERTS + 1
    own_rows = lax.dynamic_slice_in_dim(tokens, lax.axis_index("tp") * row_count, row_count, 0)
    middle = (own_rows.astype(jnp.float32) + attn_sum).astype(jnp.bfloat16)
    normed_two = normed_rows(middle, norm_ffn)
    width = normed_two.shape[1]
    piece = lax.all_gather(normed_two, "ep", axis=0, tiled=True)
    mix_gate = jax.nn.sigmoid(jnp.dot(piece, dense_mix, preferred_element_type=jnp.float32))
    dense_hidden = (
        jax.nn.silu(jnp.dot(piece, dense_gate_w, preferred_element_type=jnp.float32))
        * jnp.dot(piece, dense_up_w, preferred_element_type=jnp.float32)
    ).astype(jnp.bfloat16)
    dense_terms = (
        jnp.dot(dense_hidden, dense_down_w, preferred_element_type=jnp.float32) * mix_gate[:, None]
    )
    dense_term = lax.psum_scatter(dense_terms, "ep", scatter_dimension=0, tiled=True)
    devices = lax.axis_size(("ep", "tp"))
    members = devices // EXPERTS
    expert_ids = lax.broadcasted_iota(jnp.int32, (EXPERTS, 1, 1), 0)
    matched = routes[None, :, :] == expert_ids
    present = jnp.any(matched, axis=2).astype(jnp.int32)
    share = jnp.sum(jnp.where(matched, route_weights.astype(jnp.float32)[None, :, :], 0.0), axis=2)
    ranks = running_ranks(present)
    slot_ids = lax.broadcasted_iota(jnp.int32, (EXPERTS, capacity, row_count), 1)
    selector = (present[:, None, :] == 1) & (ranks[:, None, :] == slot_ids)
    slot_rows = jnp.einsum(
        "ecr,rk->eck", selector.astype(jnp.bfloat16), normed_two, preferred_element_type=jnp.float32
    ).astype(jnp.bfloat16)
    outgoing = jnp.repeat(slot_rows, members, axis=0)
    incoming = lax.all_to_all(outgoing, ("ep", "tp"), split_axis=0, concat_axis=0, tiled=True)
    slot_rows = incoming.reshape(devices * capacity, width)
    expert_hidden = (
        jax.nn.silu(jnp.dot(slot_rows, expert_gate, preferred_element_type=jnp.float32))
        * jnp.dot(slot_rows, expert_up, preferred_element_type=jnp.float32)
    ).astype(jnp.bfloat16)
    expert_result = jnp.dot(expert_hidden, expert_down, preferred_element_type=jnp.float32).reshape(
        devices, capacity, width
    )
    back = lax.all_to_all(
        expert_result.astype(jnp.bfloat16), ("ep", "tp"), split_axis=0, concat_axis=0, tiled=True
    ).astype(expert_result.dtype)
    per_expert = jnp.sum(back.reshape(EXPERTS, members, capacity, width), axis=1)
    expert_term = jnp.einsum("ecr,eck,er->rk", selector.astype(jnp.float32), per_expert, share)
    layer_out = (middle.astype(jnp.float32) + expert_term + dense_term).astype(jnp.bfloat16)
    return (layer_out, new_keys, new_values)


def solution(mesh):
    placed = (
        P("ep", None),
        P(),
        P(None, "tp"),
        P(None, "tp"),
        P(None, "tp"),
        P("tp", None),
        P("tp"),
        P("ep", None, "tp"),
        P("ep", None, "tp"),
        P("ep"),
        P(),
        P(None, ("ep", "tp")),
        P(None, ("ep", "tp")),
        P(("ep", "tp"), None),
        P(None, "ep"),
        P(None, "ep"),
        P("ep", None),
        P(),
        P(("ep", "tp"), None),
        P(("ep", "tp"), None),
    )
    return jax.shard_map(
        shards,
        mesh=mesh,
        in_specs=placed,
        out_specs=(P(("ep", "tp"), None), P("ep", "tp"), P("ep", "tp")),
        check_vma=False,
    )
```

profile of v0, /device:TPU:0, one launch (start us, length us, event | category | flops | bytes accessed | tf_op | source)
XLA Modules:
  0.0 201.0 jit_solution(5162440769318501514)
XLA Ops:
  8.3 2.9 %convolution_convert_fusion.4 = bf16[16,1024]{1,0:T(8,128)(2,1)S(1)} fusion(bf16[2048,1024]{1,0:T(8,128)(2,1)} %param.22, bf16[16,2048]{1,0:T(8,128)(2,1)} %param.20, f32[2048]{0:T(1024)} %param.21, f32[16]{0:T(128)S(1)} %add_rsqrt_fusion.1), kind=kOutput, calls=%fused_computation.17 | convolution fusion | flops 67256320 | bytes 4300864 | tf_op jit(solution)/shard_map/dot_general | solution.py:75
  11.4 6.4 %copy.57 = bf16[16,1024,128]{1,2,0:T(8,128)(2,1)} copy(bf16[16,1024,128]{2,1,0:T(8,128)(2,1)} %param.27) | data formatting | bytes 8388608 | tf_op args[7]
  18.0 2.8 %fusion.4 = f32[16,2,8,1024]{3,2,1,0:T(8,128)S(1)} fusion(bf16[16,2,8,64]{3,2,1,0:T(8,128)(2,1)S(1)} %reshape.82, bf16[16,1024,2,64]{1,3,2,0:T(8,128)(2,1)} %bitcast.71, f32[2,8]{1,0:T(2,128)S(1)} %add.75), kind=kOutput, calls=%fused_computation.13 | convolution fusion | flops 34078720 | bytes 5275712 | tf_op jit(solution)/shard_map/bgrd,bsgd->bgrs/dot_general | solution.py:81
  22.5 1.7 fusion.19
  24.1 2.8 %copy.74 = f32[16,2,8,8,1]{3,2,1,0,4:T(8,128)S(1)} copy(f32[16,2,8,8,1]{4,3,2,1,0:T(8,128)} %bitcast.73) | data formatting | bytes 16384 | tf_op jit(solution)/shard_map/squeeze | solution.py:28
  27.1 2.6 %add_subtract_fusion = f32[16,2,8,8,128]{4,3,2,1,0:T(8,128)} fusion(f32[16,2,8,8,128]{4,3,2,1,0:T(8,128)} %fusion.19, f32[16,2,8,8,128]{4,2,3,1,0:T(8,128)S(1)} %fusion.18, f32[16,2,8,8]{3,2,1,0:T(8,128)S(1)} %fusion.34), kind=kLoop, calls=%fused_computation.36 | loop fusion | flops 524288 | bytes 3153920 | tf_op jit(solution)/shard_map/sub | solution.py:34
  29.7 2.4 %reshape.85 = f32[16,2,8,1024]{3,2,1,0:T(8,128)} reshape(f32[16,2,8,8,128]{4,3,2,1,0:T(8,128)} %add_subtract_fusion) | data formatting | bytes 2097152 | tf_op jit(solution)/shard_map/reshape | solution.py:34
  32.1 6.5 %copy.62 = bf16[16,1024,128]{1,2,0:T(8,128)(2,1)} copy(bf16[16,1024,128]{2,1,0:T(8,128)(2,1)} %param.28) | data formatting | bytes 8388608 | tf_op args[8]
  38.6 3.8 %convolution_convert_fusion.3 = bf16[16,2,8,64]{3,2,1,0:T(8,128)(2,1)S(1)} fusion(bf16[16,1024,2,64]{1,3,2,0:T(8,128)(2,1)} %bitcast.72, f32[16,2,8,1024]{3,2,1,0:T(8,128)} %reshape.85, f32[16,2,8,1024]{3,2,1,0:T(8,128)S(1)} %copy-done.2, pred[16,1024]{1,0:T(8,128)(4,1)S(1)} %iota_compare_fusion.1), kind=kOutput, calls=%fused_computation.16 | convolution fusion | flops 36454400 | bytes 6340608 | tf_op jit(solution)/shard_map/bgrs,bsgd->bgrd/dot_general | solution.py:92
  42.5 3.5 %convolution_convert_fusion.2 = bf16[16,2048]{1,0:T(8,128)(2,1)} fusion(bf16[16,1024]{1,0:T(8,128)(2,1)S(1)} %reshape.87, bf16[1024,2048]{1,0:T(8,128)(2,1)} %param.25), kind=kOutput, calls=%fused_computation.7 | convolution fusion | flops 67141632 | bytes 4292608 | tf_op jit(solution)/shard_map/dot_general | solution.py:96
  46.4 10.1 %reduce-scatter.3.cloned.1.call-done = bf16[8,2048]{1,0:T(8,128)(2,1)} async-done(((bf16[16,2048]{1,0:T(8,128)(2,1)}), bf16[8,2048]{1,0:T(8,128)(2,1)}) %reduce-scatter.3.cloned.1.call-update) | async-done | bytes 32784 | tf_op jit(solution)/shard_map/reduce_scatter | solution.py:97
  57.4 44.0 %all_gather.3 = bf16[128,2048]{1,0:T(8,128)(2,1)S(1)} all-gather(bf16[8,2048]{1,0:T(8,128)(2,1)S(1)} %fusion.39), channel_id=1, replica_groups=mesh['ep'=16,'tp'=2] {'ep'}, dimensions={0}, use_global_device_ids=true | all-gather | bytes 557056 | tf_op jit(solution)/shard_map/all_gather | solution.py:106
  102.7 2.6 %all-to-all-start = ((bf16[32,3,2048]{2,1,0:T(4,128)(2,1)}), bf16[32,3,2048]{2,1,0:T(4,128)(2,1)S(1)}, u32[]{:S(2)}, u32[]{:S(2)}) async-start(bf16[32,3,2048]{2,1,0:T(4,128)(2,1)} %bitcast.11), calls=%async_computation.1 | async-start | bytes 1048576 | tf_op jit(solution)/shard_map/all_to_all | solution.py:129
  105.8 2.2 %fusion.65 = f32[128,448]{0,1:T(8,128)S(1)} fusion(bf16[128,2048]{1,0:T(8,128)(2,1)S(1)} %all_gather.3, bf16[2048,448]{0,1:T(8,128)(2,1)} %param.34), kind=kOutput, calls=%fused_computation.91 | convolution fusion | flops 234881024 | bytes 2588672 | tf_op jit(solution)/shard_map/dot_general | solution.py:109
  108.0 4.0 %convolution_multiply_fusion = f32[128,2048]{1,0:T(8,128)} fusion(bf16[448,2048]{1,0:T(8,128)(2,1)S(1)} %copy-done, bf16[128,2048]{1,0:T(8,128)(2,1)S(1)} %all_gather.3, bf16[2048,448]{0,1:T(8,128)(2,1)} %param.35, f32[128]{0:T(128)S(1)} %fusion.10, f32[128,448]{0,1:T(8,128)S(1)} %fusion.65), kind=kOutput, calls=%fused_computation.2 | convolution fusion | flops 470368256 | bytes 5472768 | tf_op jit(solution)/shard_map/dot_general | solution.py:113
  112.0 8.9 %all-to-all-done = bf16[32,3,2048]{2,1,0:T(4,128)(2,1)S(1)} async-done(((bf16[32,3,2048]{2,1,0:T(4,128)(2,1)}), bf16[32,3,2048]{2,1,0:T(4,128)(2,1)S(1)}, u32[]{:S(2)}, u32[]{:S(2)}) %all-to-all-start) | async-done | bytes 393248 | tf_op jit(solution)/shard_map/all_to_all | solution.py:129
  121.3 4.4 %fusion.64 = f32[96,1792]{1,0:T(8,128)S(1)} fusion(bf16[96,2048]{1,0:T(8,128)(2,1)S(1)} %reshape.89, bf16[2048,1792]{1,0:T(8,128)(2,1)} %param.31), kind=kOutput, calls=%fused_computation.90 | convolution fusion | flops 704643072 | bytes 8421376 | tf_op jit(solution)/shard_map/dot_general | solution.py:132
  125.7 7.8 %convolution_convert_fusion = bf16[96,2048]{1,0:T(8,128)(2,1)S(1)} fusion(bf16[1792,2048]{1,0:T(8,128)(2,1)} %param.33, bf16[96,2048]{1,0:T(8,128)(2,1)S(1)} %reshape.89, bf16[2048,1792]{1,0:T(8,128)(2,1)} %param.32, f32[96,1792]{1,0:T(8,128)S(1)} %fusion.64), kind=kOutput, calls=%fused_computation.5 | convolution fusion | flops 1410514944 | bytes 16154624 | tf_op jit(solution)/shard_map/dot_general | solution.py:135
  134.6 2.9 %all-to-all-start.1 = ((bf16[32,3,2048]{2,1,0:T(4,128)(2,1)}), bf16[32,3,2048]{2,1,0:T(4,128)(2,1)S(1)}, u32[]{:S(2)}, u32[]{:S(2)}) async-start(bf16[32,3,2048]{2,1,0:T(4,128)(2,1)} %convert_element_type.98), calls=%async_computation.2 | async-start | bytes 1048576 | tf_op jit(solution)/shard_map/all_to_all | solution.py:138
  137.6 1.9 convolution_convert_fusion.5
  139.5 1.9 convolution_convert_fusion.6
  141.4 13.6 %all-to-all-done.1 = bf16[32,3,2048]{2,1,0:T(4,128)(2,1)S(1)} async-done(((bf16[32,3,2048]{2,1,0:T(4,128)(2,1)}), bf16[32,3,2048]{2,1,0:T(4,128)(2,1)S(1)}, u32[]{:S(2)}, u32[]{:S(2)}) %all-to-all-start.1) | async-done | bytes 393248 | tf_op jit(solution)/shard_map/all_to_all | solution.py:138
  155.2 37.3 %reduce-scatter.5.cloned.1.call-done = f32[8,2048]{1,0:T(8,128)} async-done(((f32[128,2048]{1,0:T(8,128)}), f32[8,2048]{1,0:T(8,128)}) %reduce-scatter.5.cloned.1.call-update) | async-done | bytes 65552 | tf_op jit(solution)/shard_map/reduce_scatter | solution.py:115
  192.5 1.7 fusion.3
  (53 shorter events, 8.3 us)
Async XLA Ops:
  7.2 100.8 %copy-start = (bf16[448,2048]{1,0:T(8,128)(2,1)S(1)}, bf16[448,2048]{1,0:T(8,128)(2,1)}, u32[]{:S(2)}) copy-start(bf16[448,2048]{1,0:T(8,128)(2,1)} %param.36) | copy-start | bytes 5505028
  7.2 49.2 %reduce-scatter.3.cloned.1.call-start = ((), (), s32[]{:S(2)}) async-start(), calls=%async_computation.4 | async-start | bytes 98304 | tf_op jit(solution)/shard_map/reduce_scatter | solution.py:97
  11.4 6.4 %copy-start.9 = (f32[16]{0:T(128)S(1)}, f32[16]{0:T(128)}, u32[]{:S(2)}) copy-start(f32[16]{0:T(128)} %param.26) | copy-start | bytes 196
  11.4 6.5 %copy-start.8 = (s32[16]{0:T(128)S(1)}, s32[16]{0:T(128)}, u32[]{:S(2)}) copy-start(s32[16]{0:T(128)} %param.29) | copy-start | bytes 196
  20.8 1.0 copy-start.1
  32.1 6.5 %copy-start.2 = (f32[16,2,8,1024]{3,2,1,0:T(8,128)S(1)}, f32[16,2,8,1024]{3,2,1,0:T(8,128)}, u32[]{:S(2)}) copy-start(f32[16,2,8,1024]{3,2,1,0:T(8,128)} %copy-done.1) | copy-start | bytes 3145732
  38.6 7.4 %copy-start.7 = (s32[8,2]{0,1:T(2,128)S(1)}, s32[8,2]{0,1:T(2,128)}, u32[]{:S(2)}) copy-start(s32[8,2]{0,1:T(2,128)} %param.38) | copy-start | bytes 196
  38.6 7.7 %copy-start.6 = (bf16[2048]{0:T(1024)(128)(2,1)S(1)}, bf16[2048]{0:T(1024)(128)(2,1)}, u32[]{:S(2)}) copy-start(bf16[2048]{0:T(1024)(128)(2,1)} %param.37) | copy-start | bytes 12292
  38.6 17.8 %copy-start.3 = (bf16[16,2048]{1,0:T(8,128)(2,1)S(1)}, bf16[16,2048]{1,0:T(8,128)(2,1)}, u32[]{:S(2)}) copy-start(bf16[16,2048]{1,0:T(8,128)(2,1)} %param.20) | copy-start | bytes 196612
  38.6 18.7 %copy-start.5 = (f32[2048]{0:T(1024)S(1)}, f32[2048]{0:T(1024)}, u32[]{:S(2)}) copy-start(f32[2048]{0:T(1024)} %param.30) | copy-start | bytes 24580
  102.7 18.2 %all-to-all-start = ((bf16[32,3,2048]{2,1,0:T(4,128)(2,1)}), bf16[32,3,2048]{2,1,0:T(4,128)(2,1)S(1)}, u32[]{:S(2)}, u32[]{:S(2)}) async-start(bf16[32,3,2048]{2,1,0:T(4,128)(2,1)} %bitcast.11), calls=%async_computation.1 | async-start | bytes 1048576 | tf_op jit(solution)/shard_map/all_to_all | solution.py:129
  105.3 87.1 %reduce-scatter.5.cloned.1.call-start = ((), (), s32[]{:S(2)}) async-start(), calls=%async_computation.5 | async-start | bytes 1114112 | tf_op jit(solution)/shard_map/reduce_scatter | solution.py:115
  125.7 11.8 %copy-start.10 = (bf16[8,2]{0,1:T(2,128)(2,1)S(1)}, bf16[8,2]{0,1:T(2,128)(2,1)}, u32[]{:S(2)}) copy-start(bf16[8,2]{0,1:T(2,128)(2,1)} %param.39) | copy-start | bytes 100
  125.7 11.9 %copy-start.4 = (f32[2048]{0:T(1024)S(1)}, f32[2048]{0:T(1024)}, u32[]{:S(2)}) copy-start(f32[2048]{0:T(1024)} %param.21) | copy-start | bytes 24580
  134.6 20.3 %all-to-all-start.1 = ((bf16[32,3,2048]{2,1,0:T(4,128)(2,1)}), bf16[32,3,2048]{2,1,0:T(4,128)(2,1)S(1)}, u32[]{:S(2)}, u32[]{:S(2)}) async-start(bf16[32,3,2048]{2,1,0:T(4,128)(2,1)} %convert_element_type.98), calls=%async_computation.2 | async-start | bytes 1048576 | tf_op jit(solution)/shard_map/all_to_all | solution.py:138
Sparse Core Ops, SparseCore 0:
  46.1 10.2 reduce-scatter.2
  112.2 80.2 reduce-scatter.4
where the time goes:
time: 202 us; the launch traced here: 201 us
  waiting for transfers between devices  69.9 us (35%)
  blocking collectives  44 us (22%)
  matrix products  39.3 us (19%)
  local copies, waits for them, and re-layouts  22.1 us (11%)
  between operations  14.3 us (7%)
  starting transfers between devices  5.75 us (3%)
  other arithmetic  5.72 us (3%)
    all_gather x1, blocking collectives, shards(): piece = lax.all_gather(normed_two, 'ep', axis=0, tiled=True)  44 us
    reduce_scatter x1, waiting for transfers between devices, shards(): lax.psum_scatter(dense_terms, 'ep', scatter_dimension=0, tiled=True)  37.3 us
    unnamed x25, local copies, waits for them, and re-layouts  13.9 us
    all_to_all x1, waiting for transfers between devices, shards(): lax.all_to_all(expert_result.astype(jnp.bfloat16), ('ep', 'tp'), split_ax...  13.6 us
    reduce_scatter x1, waiting for transfers between devices, shards(): lax.psum_scatter(partial_value.astype(jnp.bfloat16), 'tp', scatter_dimens...  10.1 us
    all_to_all x1, waiting for transfers between devices, shards(): lax.all_to_all(outgoing, ('ep', 'tp'), split_axis=0, concat_axis=0, tiled...  8.92 us
    dot_general x1, matrix products, shards(): jnp.dot(expert_hidden, expert_down, preferred_element_type=jnp.float32)  7.84 us
    dot_general x1, matrix products, shards(): jnp.dot(slot_rows, expert_gate, preferred_element_type=jnp.float32)  4.37 us
  transfers between devices with their start and end apart: 4, of which 4 were waited for; matrix products, arithmetic and copies ran while one was open for 12% of the time, Pallas kernels for 0%

commit v1 on v0

--- a/solution.py
+++ b/solution.py
@@ -103,7 +103,12 @@
     middle = (own_rows.astype(jnp.float32) + attn_sum).astype(jnp.bfloat16)
     normed_two = normed_rows(middle, norm_ffn)
     width = normed_two.shape[1]
-    piece = lax.all_gather(normed_two, "ep", axis=0, tiled=True)
+    ring = [normed_two]
+    for hop in range(15):
+        ring.append(lax.ppermute(ring[-1], "ep", [(dev, (dev + 1) % 16) for dev in range(16)]))
+    piece = jnp.roll(
+        jnp.concatenate(ring[::-1], axis=0), (lax.axis_index("ep") + 1) * ring[0].shape[0], axis=0
+    )
     mix_gate = jax.nn.sigmoid(jnp.dot(piece, dense_mix, preferred_element_type=jnp.float32))
     dense_hidden = (
         jax.nn.silu(jnp.dot(piece, dense_gate_w, preferred_element_type=jnp.float32))

time: 202 us -> 299 us (1.48)
  waiting for transfers between devices: 69.9 us -> 170 us
  blocking collectives: 44 us -> 0 us
  local copies, waits for them, and re-layouts: 22.1 us -> 50.5 us
  starting transfers between devices: 5.75 us -> 13.8 us
    ppermute x0 -> x15, waiting for transfers between devices: none -> 103 us  [shards(): lax.ppermute(ring[-1], 'ep', [(dev, (dev + 1) % 16) for dev in range(16)])]
    all_gather x1 -> x0, blocking collectives: 44 us -> none  [shards(): piece = lax.all_gather(normed_two, 'ep', axis=0, tiled=True)]
    unnamed x25 -> x89, local copies, waits for them, and re-layouts: 13.9 us -> 42.3 us
    all_to_all x1, waiting for transfers between devices: 8.92 us -> 0.01 us  [shards(): lax.all_to_all(outgoing, ('ep', 'tp'), split_axis=0, concat_axis=0, tiled...]
    reduce_scatter x1, waiting for transfers between devices: 37.3 us -> 43.1 us  [shards(): lax.psum_scatter(dense_terms, 'ep', scatter_dimension=0, tiled=True)]
    all_to_all x1, starting transfers between devices: 2.6 us -> 5.98 us  [shards(): lax.all_to_all(outgoing, ('ep', 'tp'), split_axis=0, concat_axis=0, tiled...]
  transfers between devices with their start and end apart: 4 -> 19, of which waited for: 4 -> 17; matrix products, arithmetic and copies ran while one was open for 12% -> 17% of each run, Pallas kernels for 0% -> 0%
where the time goes in v1:
time: 299 us; the launch traced here: 296 us
  waiting for transfers between devices  170 us (57%)
  local copies, waits for them, and re-layouts  50.5 us (17%)
  matrix products  40.7 us (14%)
  between operations  14.4 us (5%)
  starting transfers between devices  13.8 us (5%)
  other arithmetic  7.18 us (2%)
    ppermute x15, waiting for transfers between devices, shards(): lax.ppermute(ring[-1], 'ep', [(dev, (dev + 1) % 16) for dev in range(16)])  103 us
    reduce_scatter x1, waiting for transfers between devices, shards(): lax.psum_scatter(dense_terms, 'ep', scatter_dimension=0, tiled=True)  43.1 us
    unnamed x89, local copies, waits for them, and re-layouts  42.3 us
    all_to_all x1, waiting for transfers between devices, shards(): lax.all_to_all(expert_result.astype(jnp.bfloat16), ('ep', 'tp'), split_ax...  13.6 us
    reduce_scatter x1, waiting for transfers between devices, shards(): lax.psum_scatter(partial_value.astype(jnp.bfloat16), 'tp', scatter_dimens...  10.4 us
    dot_general x1, matrix products, shards(): jnp.dot(expert_hidden, expert_down, preferred_element_type=jnp.float32)  7.84 us
    all_to_all x1, starting transfers between devices, shards(): lax.all_to_all(outgoing, ('ep', 'tp'), split_axis=0, concat_axis=0, tiled...  5.98 us
  transfers between devices with their start and end apart: 19, of which 17 were waited for; matrix products, arithmetic and copies ran while one was open for 17% of the time, Pallas kernels for 0%

profile of v1, /device:TPU:0, one launch (start us, length us, event | category | flops | bytes accessed | tf_op | source)
XLA Modules:
  0.0 296.2 jit_solution(12173232334426916049)
XLA Ops:
  11.9 6.4 %copy.57 = bf16[16,1024,128]{1,2,0:T(8,128)(2,1)} copy(bf16[16,1024,128]{2,1,0:T(8,128)(2,1)} %param.27) | data formatting | bytes 8388608 | tf_op args[7]
  32.7 6.5 %copy.62 = bf16[16,1024,128]{1,2,0:T(8,128)(2,1)} copy(bf16[16,1024,128]{2,1,0:T(8,128)(2,1)} %param.28) | data formatting | bytes 8388608 | tf_op args[8]
  46.6 10.4 %reduce-scatter.3.cloned.1.call-done = bf16[8,2048]{1,0:T(8,128)(2,1)} async-done(((bf16[16,2048]{1,0:T(8,128)(2,1)}), bf16[8,2048]{1,0:T(8,128)(2,1)}) %reduce-scatter.3.cloned.1.call-update) | async-done | bytes 32784 | tf_op jit(solution)/shard_map/reduce_scatter | solution.py:97
  60.2 5.8 %collective-permute-done = bf16[8,2048]{1,0:T(8,128)(2,1)S(1)} collective-permute-done((bf16[8,2048]{1,0:T(8,128)(2,1)S(1)}, bf16[8,2048]{1,0:T(8,128)(2,1)S(1)}, u32[]{:S(2)}, u32[]{:S(2)}) %collective-permute-start) | collective-permute-done | bytes 32800 | tf_op jit(solution)/shard_map/ppermute | solution.py:108
  66.0 7.5 %collective-permute-done.1 = bf16[8,2048]{1,0:T(8,128)(2,1)S(1)} collective-permute-done((bf16[8,2048]{1,0:T(8,128)(2,1)S(1)}, bf16[8,2048]{1,0:T(8,128)(2,1)S(1)}, u32[]{:S(2)}, u32[]{:S(2)}) %collective-permute-start.1) | collective-permute-done | bytes 32800 | tf_op jit(solution)/shard_map/ppermute | solution.py:108
  74.2 7.5 %collective-permute-done.2 = bf16[8,2048]{1,0:T(8,128)(2,1)S(1)} collective-permute-done((bf16[8,2048]{1,0:T(8,128)(2,1)S(1)}, bf16[8,2048]{1,0:T(8,128)(2,1)S(1)}, u32[]{:S(2)}, u32[]{:S(2)}) %collective-permute-start.2) | collective-permute-done | bytes 32800 | tf_op jit(solution)/shard_map/ppermute | solution.py:108
  82.3 7.5 %collective-permute-done.3 = bf16[8,2048]{1,0:T(8,128)(2,1)S(1)} collective-permute-done((bf16[8,2048]{1,0:T(8,128)(2,1)S(1)}, bf16[8,2048]{1,0:T(8,128)(2,1)S(1)}, u32[]{:S(2)}, u32[]{:S(2)}) %collective-permute-start.3) | collective-permute-done | bytes 32800 | tf_op jit(solution)/shard_map/ppermute | solution.py:108
  90.4 7.5 %collective-permute-done.4 = bf16[8,2048]{1,0:T(8,128)(2,1)S(1)} collective-permute-done((bf16[8,2048]{1,0:T(8,128)(2,1)S(1)}, bf16[8,2048]{1,0:T(8,128)(2,1)S(1)}, u32[]{:S(2)}, u32[]{:S(2)}) %collective-permute-start.4) | collective-permute-done | bytes 32800 | tf_op jit(solution)/shard_map/ppermute | solution.py:108
  98.5 7.5 %collective-permute-done.5 = bf16[8,2048]{1,0:T(8,128)(2,1)S(1)} collective-permute-done((bf16[8,2048]{1,0:T(8,128)(2,1)S(1)}, bf16[8,2048]{1,0:T(8,128)(2,1)S(1)}, u32[]{:S(2)}, u32[]{:S(2)}) %collective-permute-start.5) | collective-permute-done | bytes 32800 | tf_op jit(solution)/shard_map/ppermute | solution.py:108
  106.6 7.5 %collective-permute-done.6 = bf16[8,2048]{1,0:T(8,128)(2,1)S(1)} collective-permute-done((bf16[8,2048]{1,0:T(8,128)(2,1)S(1)}, bf16[8,2048]{1,0:T(8,128)(2,1)S(1)}, u32[]{:S(2)}, u32[]{:S(2)}) %collective-permute-start.6) | collective-permute-done | bytes 32800 | tf_op jit(solution)/shard_map/ppermute | solution.py:108
  114.7 7.5 %collective-permute-done.7 = bf16[8,2048]{1,0:T(8,128)(2,1)S(1)} collective-permute-done((bf16[8,2048]{1,0:T(8,128)(2,1)S(1)}, bf16[8,2048]{1,0:T(8,128)(2,1)S(1)}, u32[]{:S(2)}, u32[]{:S(2)}) %collective-permute-start.7) | collective-permute-done | bytes 32800 | tf_op jit(solution)/shard_map/ppermute | solution.py:108
  122.8 7.5 %collective-permute-done.8 = bf16[8,2048]{1,0:T(8,128)(2,1)S(1)} collective-permute-done((bf16[8,2048]{1,0:T(8,128)(2,1)S(1)}, bf16[8,2048]{1,0:T(8,128)(2,1)S(1)}, u32[]{:S(2)}, u32[]{:S(2)}) %collective-permute-start.8) | collective-permute-done | bytes 32800 | tf_op jit(solution)/shard_map/ppermute | solution.py:108
  131.0 7.5 %collective-permute-done.9 = bf16[8,2048]{1,0:T(8,128)(2,1)S(1)} collective-permute-done((bf16[8,2048]{1,0:T(8,128)(2,1)S(1)}, bf16[8,2048]{1,0:T(8,128)(2,1)S(1)}, u32[]{:S(2)}, u32[]{:S(2)}) %collective-permute-start.9) | collective-permute-done | bytes 32800 | tf_op jit(solution)/shard_map/ppermute | solution.py:108
  139.1 7.5 %collective-permute-done.10 = bf16[8,2048]{1,0:T(8,128)(2,1)S(1)} collective-permute-done((bf16[8,2048]{1,0:T(8,128)(2,1)S(1)}, bf16[8,2048]{1,0:T(8,128)(2,1)S(1)}, u32[]{:S(2)}, u32[]{:S(2)}) %collective-permute-start.10) | collective-permute-done | bytes 32800 | tf_op jit(solution)/shard_map/ppermute | solution.py:108
  146.6 7.5 %collective-permute-done.11 = bf16[8,2048]{1,0:T(8,128)(2,1)S(1)} collective-permute-done((bf16[8,2048]{1,0:T(8,128)(2,1)S(1)}, bf16[8,2048]{1,0:T(8,128)(2,1)S(1)}, u32[]{:S(2)}, u32[]{:S(2)}) %collective-permute-start.11) | collective-permute-done | bytes 32800 | tf_op jit(solution)/shard_map/ppermute | solution.py:108
  154.2 7.4 %collective-permute-done.12 = bf16[8,2048]{1,0:T(8,128)(2,1)S(1)} collective-permute-done((bf16[8,2048]{1,0:T(8,128)(2,1)S(1)}, bf16[8,2048]{1,0:T(8,128)(2,1)S(1)}, u32[]{:S(2)}, u32[]{:S(2)}) %collective-permute-start.12) | collective-permute-done | bytes 32800 | tf_op jit(solution)/shard_map/ppermute | solution.py:108
  162.4 6.7 %collective-permute-done.13 = bf16[8,2048]{1,0:T(8,128)(2,1)S(1)} collective-permute-done((bf16[8,2048]{1,0:T(8,128)(2,1)S(1)}, bf16[8,2048]{1,0:T(8,128)(2,1)S(1)}, u32[]{:S(2)}, u32[]{:S(2)}) %collective-permute-start.13) | collective-permute-done | bytes 32800 | tf_op jit(solution)/shard_map/ppermute | solution.py:108
  170.5 6.0 %all-to-all-start = ((bf16[32,3,2048]{2,1,0:T(4,128)(2,1)}), bf16[32,3,2048]{2,1,0:T(4,128)(2,1)S(1)}, u32[]{:S(2)}, u32[]{:S(2)}) async-start(bf16[32,3,2048]{2,1,0:T(4,128)(2,1)} %bitcast.11), calls=%async_computation.1 | async-start | bytes 1048576 | tf_op jit(solution)/shard_map/all_to_all | solution.py:134
  203.3 4.0 %convolution_multiply_fusion = f32[128,2048]{1,0:T(8,128)} fusion(bf16[448,2048]{1,0:T(8,128)(2,1)S(1)} %copy-done, f32[128]{0:T(128)S(1)} %fusion.9, f32[128,448]{0,1:T(8,128)} %fusion.24, bf16[2048,448]{0,1:T(8,128)(2,1)} %param.34, bf16[256,2048]{1,0:T(8,128)(2,1)S(1)} %constant_dynamic-update-slice_fusion, s32[]{:T(128)S(6)} %select_n.42), kind=kOutput, calls=%fused_computation.2 | convolution fusion | flops 470368256 | bytes 5472772 | tf_op jit(solution)/shard_map/dot_general | solution.py:118
  207.8 4.4 %fusion.71 = f32[96,1792]{1,0:T(8,128)S(1)} fusion(bf16[96,2048]{1,0:T(8,128)(2,1)S(1)} %reshape.89, bf16[2048,1792]{1,0:T(8,128)(2,1)} %param.31), kind=kOutput, calls=%fused_computation.124 | convolution fusion | flops 704643072 | bytes 8421376 | tf_op jit(solution)/shard_map/dot_general | solution.py:137
  212.2 7.8 %convolution_convert_fusion = bf16[96,2048]{1,0:T(8,128)(2,1)S(1)} fusion(bf16[1792,2048]{1,0:T(8,128)(2,1)} %param.33, bf16[96,2048]{1,0:T(8,128)(2,1)S(1)} %reshape.89, bf16[2048,1792]{1,0:T(8,128)(2,1)} %param.32, f32[96,1792]{1,0:T(8,128)S(1)} %fusion.71), kind=kOutput, calls=%fused_computation.5 | convolution fusion | flops 1410514944 | bytes 16154624 | tf_op jit(solution)/shard_map/dot_general | solution.py:140
  221.0 5.8 %all-to-all-start.1 = ((bf16[32,3,2048]{2,1,0:T(4,128)(2,1)}), bf16[32,3,2048]{2,1,0:T(4,128)(2,1)S(1)}, u32[]{:S(2)}, u32[]{:S(2)}) async-start(bf16[32,3,2048]{2,1,0:T(4,128)(2,1)} %convert_element_type.98), calls=%async_computation.2 | async-start | bytes 1048576 | tf_op jit(solution)/shard_map/all_to_all | solution.py:143
  230.8 13.6 %all-to-all-done.1 = bf16[32,3,2048]{2,1,0:T(4,128)(2,1)S(1)} async-done(((bf16[32,3,2048]{2,1,0:T(4,128)(2,1)}), bf16[32,3,2048]{2,1,0:T(4,128)(2,1)S(1)}, u32[]{:S(2)}, u32[]{:S(2)}) %all-to-all-start.1) | async-done | bytes 393248 | tf_op jit(solution)/shard_map/all_to_all | solution.py:143
  244.6 43.1 %reduce-scatter.5.cloned.1.call-done = f32[8,2048]{1,0:T(8,128)} async-done(((f32[128,2048]{1,0:T(8,128)}), f32[8,2048]{1,0:T(8,128)}) %reduce-scatter.5.cloned.1.call-update) | async-done | bytes 65552 | tf_op jit(solution)/shard_map/reduce_scatter | solution.py:120
  (148 shorter events, 71.3 us)
Async XLA Ops:
  7.2 196.2 %copy-start = (bf16[448,2048]{1,0:T(8,128)(2,1)S(1)}, bf16[448,2048]{1,0:T(8,128)(2,1)}, u32[]{:S(2)}) copy-start(bf16[448,2048]{1,0:T(8,128)(2,1)} %param.36) | copy-start | bytes 5505028
  7.2 49.8 %reduce-scatter.3.cloned.1.call-start = ((), (), s32[]{:S(2)}) async-start(), calls=%async_computation.4 | async-start | bytes 98304 | tf_op jit(solution)/shard_map/reduce_scatter | solution.py:97
  39.2 107.4 %copy-start.23 = (s32[8,2]{0,1:T(2,128)S(1)}, s32[8,2]{0,1:T(2,128)}, u32[]{:S(2)}) copy-start(s32[8,2]{0,1:T(2,128)} %param.38) | copy-start | bytes 196
  39.2 122.4 %copy-start.22 = (bf16[2048]{0:T(1024)(128)(2,1)S(1)}, bf16[2048]{0:T(1024)(128)(2,1)}, u32[]{:S(2)}) copy-start(bf16[2048]{0:T(1024)(128)(2,1)} %param.37) | copy-start | bytes 12292
  58.5 7.5 %collective-permute-start = (bf16[8,2048]{1,0:T(8,128)(2,1)S(1)}, bf16[8,2048]{1,0:T(8,128)(2,1)S(1)}, u32[]{:S(2)}, u32[]{:S(2)}) collective-permute-start(bf16[8,2048]{1,0:T(8,128)(2,1)S(1)} %fusion.42), channel_id=1, source_target_pairs={{0,2},{2,4},{4,6},{6,8},{8,10},{10,12},{12,14},{14,16},{16,18},{18... | collective-permute-start | bytes 98312 | tf_op jit(solution)/shard_map/ppermute | solution.py:108
  66.0 7.5 %collective-permute-start.1 = (bf16[8,2048]{1,0:T(8,128)(2,1)S(1)}, bf16[8,2048]{1,0:T(8,128)(2,1)S(1)}, u32[]{:S(2)}, u32[]{:S(2)}) collective-permute-start(bf16[8,2048]{1,0:T(8,128)(2,1)S(1)} %collective-permute-done), channel_id=1, source_target_pairs={{0,2},{2,4},{4,6},{6,8},{8,10},{10,12},{12,14},{14,16},{16,18},{18... | collective-permute-start | bytes 98312 | tf_op jit(solution)/shard_map/ppermute | solution.py:108
  74.2 7.5 %collective-permute-start.2 = (bf16[8,2048]{1,0:T(8,128)(2,1)S(1)}, bf16[8,2048]{1,0:T(8,128)(2,1)S(1)}, u32[]{:S(2)}, u32[]{:S(2)}) collective-permute-start(bf16[8,2048]{1,0:T(8,128)(2,1)S(1)} %collective-permute-done.1), channel_id=1, source_target_pairs={{0,2},{2,4},{4,6},{6,8},{8,10},{10,12},{12,14},{14,16},{16,18},{18... | collective-permute-start | bytes 98312 | tf_op jit(solution)/shard_map/ppermute | solution.py:108
  82.3 7.5 %collective-permute-start.3 = (bf16[8,2048]{1,0:T(8,128)(2,1)S(1)}, bf16[8,2048]{1,0:T(8,128)(2,1)S(1)}, u32[]{:S(2)}, u32[]{:S(2)}) collective-permute-start(bf16[8,2048]{1,0:T(8,128)(2,1)S(1)} %collective-permute-done.2), channel_id=1, source_target_pairs={{0,2},{2,4},{4,6},{6,8},{8,10},{10,12},{12,14},{14,16},{16,18},{18... | collective-permute-start | bytes 98312 | tf_op jit(solution)/shard_map/ppermute | solution.py:108
  90.4 7.5 %collective-permute-start.4 = (bf16[8,2048]{1,0:T(8,128)(2,1)S(1)}, bf16[8,2048]{1,0:T(8,128)(2,1)S(1)}, u32[]{:S(2)}, u32[]{:S(2)}) collective-permute-start(bf16[8,2048]{1,0:T(8,128)(2,1)S(1)} %collective-permute-done.3), channel_id=1, source_target_pairs={{0,2},{2,4},{4,6},{6,8},{8,10},{10,12},{12,14},{14,16},{16,18},{18... | collective-permute-start | bytes 98312 | tf_op jit(solution)/shard_map/ppermute | solution.py:108
  98.5 7.5 %collective-permute-start.5 = (bf16[8,2048]{1,0:T(8,128)(2,1)S(1)}, bf16[8,2048]{1,0:T(8,128)(2,1)S(1)}, u32[]{:S(2)}, u32[]{:S(2)}) collective-permute-start(bf16[8,2048]{1,0:T(8,128)(2,1)S(1)} %collective-permute-done.4), channel_id=1, source_target_pairs={{0,2},{2,4},{4,6},{6,8},{8,10},{10,12},{12,14},{14,16},{16,18},{18... | collective-permute-start | bytes 98312 | tf_op jit(solution)/shard_map/ppermute | solution.py:108
  106.6 7.5 %collective-permute-start.6 = (bf16[8,2048]{1,0:T(8,128)(2,1)S(1)}, bf16[8,2048]{1,0:T(8,128)(2,1)S(1)}, u32[]{:S(2)}, u32[]{:S(2)}) collective-permute-start(bf16[8,2048]{1,0:T(8,128)(2,1)S(1)} %collective-permute-done.5), channel_id=1, source_target_pairs={{0,2},{2,4},{4,6},{6,8},{8,10},{10,12},{12,14},{14,16},{16,18},{18... | collective-permute-start | bytes 98312 | tf_op jit(solution)/shard_map/ppermute | solution.py:108
  114.7 7.5 %collective-permute-start.7 = (bf16[8,2048]{1,0:T(8,128)(2,1)S(1)}, bf16[8,2048]{1,0:T(8,128)(2,1)S(1)}, u32[]{:S(2)}, u32[]{:S(2)}) collective-permute-start(bf16[8,2048]{1,0:T(8,128)(2,1)S(1)} %collective-permute-done.6), channel_id=1, source_target_pairs={{0,2},{2,4},{4,6},{6,8},{8,10},{10,12},{12,14},{14,16},{16,18},{18... | collective-permute-start | bytes 98312 | tf_op jit(solution)/shard_map/ppermute | solution.py:108
  122.8 7.5 %collective-permute-start.8 = (bf16[8,2048]{1,0:T(8,128)(2,1)S(1)}, bf16[8,2048]{1,0:T(8,128)(2,1)S(1)}, u32[]{:S(2)}, u32[]{:S(2)}) collective-permute-start(bf16[8,2048]{1,0:T(8,128)(2,1)S(1)} %collective-permute-done.7), channel_id=1, source_target_pairs={{0,2},{2,4},{4,6},{6,8},{8,10},{10,12},{12,14},{14,16},{16,18},{18... | collective-permute-start | bytes 98312 | tf_op jit(solution)/shard_map/ppermute | solution.py:108
  131.0 7.5 %collective-permute-start.9 = (bf16[8,2048]{1,0:T(8,128)(2,1)S(1)}, bf16[8,2048]{1,0:T(8,128)(2,1)S(1)}, u32[]{:S(2)}, u32[]{:S(2)}) collective-permute-start(bf16[8,2048]{1,0:T(8,128)(2,1)S(1)} %collective-permute-done.8), channel_id=1, source_target_pairs={{0,2},{2,4},{4,6},{6,8},{8,10},{10,12},{12,14},{14,16},{16,18},{18... | collective-permute-start | bytes 98312 | tf_op jit(solution)/shard_map/ppermute | solution.py:108
  139.1 7.5 %collective-permute-start.10 = (bf16[8,2048]{1,0:T(8,128)(2,1)S(1)}, bf16[8,2048]{1,0:T(8,128)(2,1)S(1)}, u32[]{:S(2)}, u32[]{:S(2)}) collective-permute-start(bf16[8,2048]{1,0:T(8,128)(2,1)S(1)} %collective-permute-done.9), channel_id=1, source_target_pairs={{0,2},{2,4},{4,6},{6,8},{8,10},{10,12},{12,14},{14,16},{16,18},{18... | collective-permute-start | bytes 98312 | tf_op jit(solution)/shard_map/ppermute | solution.py:108
  146.6 30.1 %copy-start.13 = (bf16[8,2048]{1,0:T(8,128)(2,1)}, bf16[8,2048]{1,0:T(8,128)(2,1)S(1)}, u32[]{:S(2)}) copy-start(bf16[8,2048]{1,0:T(8,128)(2,1)S(1)} %collective-permute-done.10) | copy-start | bytes 98308
  146.6 7.5 %collective-permute-start.11 = (bf16[8,2048]{1,0:T(8,128)(2,1)S(1)}, bf16[8,2048]{1,0:T(8,128)(2,1)S(1)}, u32[]{:S(2)}, u32[]{:S(2)}) collective-permute-start(bf16[8,2048]{1,0:T(8,128)(2,1)S(1)} %collective-permute-done.10), channel_id=1, source_target_pairs={{0,2},{2,4},{4,6},{6,8},{8,10},{10,12},{12,14},{14,16},{16,18},{18... | collective-permute-start | bytes 98312 | tf_op jit(solution)/shard_map/ppermute | solution.py:108
  154.1 22.6 %copy-start.14 = (bf16[8,2048]{1,0:T(8,128)(2,1)}, bf16[8,2048]{1,0:T(8,128)(2,1)S(1)}, u32[]{:S(2)}) copy-start(bf16[8,2048]{1,0:T(8,128)(2,1)S(1)} %collective-permute-done.11) | copy-start | bytes 98308
  154.1 7.5 %collective-permute-start.12 = (bf16[8,2048]{1,0:T(8,128)(2,1)S(1)}, bf16[8,2048]{1,0:T(8,128)(2,1)S(1)}, u32[]{:S(2)}, u32[]{:S(2)}) collective-permute-start(bf16[8,2048]{1,0:T(8,128)(2,1)S(1)} %collective-permute-done.11), channel_id=1, source_target_pairs={{0,2},{2,4},{4,6},{6,8},{8,10},{10,12},{12,14},{14,16},{16,18},{18... | collective-permute-start | bytes 98312 | tf_op jit(solution)/shard_map/ppermute | solution.py:108
  161.6 7.5 %collective-permute-start.13 = (bf16[8,2048]{1,0:T(8,128)(2,1)S(1)}, bf16[8,2048]{1,0:T(8,128)(2,1)S(1)}, u32[]{:S(2)}, u32[]{:S(2)}) collective-permute-start(bf16[8,2048]{1,0:T(8,128)(2,1)S(1)} %collective-permute-done.12), channel_id=1, source_target_pairs={{0,2},{2,4},{4,6},{6,8},{8,10},{10,12},{12,14},{14,16},{16,18},{18... | collective-permute-start | bytes 98312 | tf_op jit(solution)/shard_map/ppermute | solution.py:108
  169.1 7.6 %collective-permute-start.14 = (bf16[8,2048]{1,0:T(8,128)(2,1)S(1)}, bf16[8,2048]{1,0:T(8,128)(2,1)}, u32[]{:S(2)}, u32[]{:S(2)}) collective-permute-start(bf16[8,2048]{1,0:T(8,128)(2,1)S(1)} %collective-permute-done.13), channel_id=1, source_target_pairs={{0,2},{2,4},{4,6},{6,8},{8,10},{10,12},{12,14},{14,16},{16,18},{18... | collective-permute-start | bytes 98312 | tf_op jit(solution)/shard_map/ppermute | solution.py:108
  170.5 36.9 %all-to-all-start = ((bf16[32,3,2048]{2,1,0:T(4,128)(2,1)}), bf16[32,3,2048]{2,1,0:T(4,128)(2,1)S(1)}, u32[]{:S(2)}, u32[]{:S(2)}) async-start(bf16[32,3,2048]{2,1,0:T(4,128)(2,1)} %bitcast.11), calls=%async_computation.1 | async-start | bytes 1048576 | tf_op jit(solution)/shard_map/all_to_all | solution.py:134
  176.5 111.2 %reduce-scatter.5.cloned.1.call-start = ((), (), s32[]{:S(2)}) async-start(), calls=%async_computation.5 | async-start | bytes 1114112 | tf_op jit(solution)/shard_map/reduce_scatter | solution.py:120
  221.0 23.3 %all-to-all-start.1 = ((bf16[32,3,2048]{2,1,0:T(4,128)(2,1)}), bf16[32,3,2048]{2,1,0:T(4,128)(2,1)S(1)}, u32[]{:S(2)}, u32[]{:S(2)}) async-start(bf16[32,3,2048]{2,1,0:T(4,128)(2,1)} %convert_element_type.98), calls=%async_computation.2 | async-start | bytes 1048576 | tf_op jit(solution)/shard_map/all_to_all | solution.py:143
  (23 other events, 146.0 us)
Sparse Core Ops, SparseCore 0:
  46.7 10.2 reduce-scatter.2
  207.5 80.1 reduce-scatter.4
